TPU v7x, 32 devices: a whole 2x2x4 slice. The times are simulated.
32 devices in a mesh: sp: 16 (over z, x, core), tp: 2 (over y).
Axes of the slice: x: 2, y: 2, z: 4, core: 2. Of those that a mesh axis runs over, the one named last changes fastest.
Arguments:
- residual: bfloat16 [4096, 2048], P(('sp', 'tp')), may hold values from -6 to 6
- query_vectors: bfloat16 [4096, 512], P('sp', 'tp'), may hold values from -6 to 6
- key_vectors: bfloat16 [4096, 512], P('sp', 'tp'), may hold values from -6 to 6
- value_vectors: bfloat16 [4096, 512], P('sp', 'tp'), may hold values from -6 to 6
- in_gate: float32 [8, 4096], P('tp', 'sp'), may hold values from -9 to 190
- forget_gate: float32 [8, 4096], P('tp', 'sp'), may hold values from -1 to 12
- documents: int32 [4096], P('sp'), may hold values from 0 to 3, never falling along the last dimension, each value on 1 to 2048 neighbouring positions
- w_out: bfloat16 [512, 2048], P('tp'), may hold values from -0.25 to 0.25
- norm_gain: bfloat16 [2048], replicated, may hold values from 0.099609375 to 1.8984375
- w_up: bfloat16 [2048, 8192], P('sp', 'tp'), may hold values from -0.125 to 0.125
- w_down: bfloat16 [8192, 2048], P('tp', 'sp'), may hold values from -0.0625 to 0.0625
Outputs:
- layer_out: bfloat16 [4096, 2048], P(('sp', 'tp'))
Inputs may be any that keep to these rules, and one draw needn't show every extreme that they name: `documents`: document numbers never fall along the positions; every document has 1 to 2048 positions.
All inputs are finite; a program needn't handle non-finite values.
Results may differ from a plain program's by a relative error of at most 0.015.
Values may be sent and summed in bfloat16 or wider, within the bound.
A program may use at most 128 MiB of HBM per device.

v0:
```python
import jax
import jax.numpy as jnp
import numpy as np
from jax import lax
from jax.sharding import Mesh, PartitionSpec as P

DOC_MOST = 2048
very_negative = -1e30
epsilon = 1e-06
SP = ("z", "g")


def combine(earlier, later):
    memory_one, top_one, decay_one, first_one, last_one = earlier
    memory_two, top_two, decay_two, first_two, last_two = later
    later_empty = first_two < 0.0
    earlier_empty = first_one < 0.0
    keep = later_empty | (first_two == last_two) & (first_two == last_one)
    decay_step = jnp.where(later_empty, 0.0, decay_two)
    top_new = jnp.where(keep, jnp.maximum(decay_step + top_one, top_two), top_two)
    scale_old = jnp.where(keep, jnp.exp(decay_step + top_one - top_new), 0.0)
    scale_new = jnp.exp(top_two - top_new)
    memory_new = scale_old[:, None, None] * memory_one + scale_new[:, None, None] * memory_two
    decay_new = jnp.where(keep, decay_one + decay_step, decay_two)
    first_new = jnp.where(earlier_empty, first_two, first_one)
    last_new = jnp.where(later_empty, last_one, last_two)
    return (memory_new, top_new, decay_new, first_new, last_new)


def pack(state):
    memory, top, decay, first, last = state
    heads, _, width = memory.shape
    row = jnp.stack(
        [top, decay, jnp.broadcast_to(first, top.shape), jnp.broadcast_to(last, top.shape)], axis=1
    )
    row = jnp.pad(row, ((0, 0), (0, width - 4)))
    return jnp.concatenate(
        [memory, row[:, None, :], jnp.zeros((heads, 6, width), jnp.float32)], axis=1
    )


def unpack(packed, present):
    rows = packed.shape[1] - 7
    row = packed[:, rows]
    memory = jnp.where(present, packed[:, :rows], 0.0)
    top = jnp.where(present, row[:, 0], very_negative)
    decay = jnp.where(present, row[:, 1], 0.0)
    first = jnp.where(present, row[0, 2], -1.0)
    last = jnp.where(present, row[0, 3], -1.0)
    return (memory, top, decay, first, last)


def shifted(state, distance, length, here):
    packed = lax.ppermute(pack(state), SP, [(i, i + distance) for i in range(length - distance)])
    return unpack(packed, here >= distance)


def on_device(
    residual,
    query_vectors,
    key_vectors,
    value_vectors,
    in_gate,
    forget_gate,
    documents,
    w_out,
    norm_gain,
    w_up,
    w_down,
):
    tok_rows = query_vectors.shape[0]
    heads = in_gate.shape[0]
    head_dim = query_vectors.shape[1] // heads
    length = lax.axis_size(SP)
    here = lax.axis_index(SP)
    tp = lax.axis_size("tp")
    me = lax.axis_index("tp")
    up_part = lax.all_to_all(w_up, "g", split_axis=1, concat_axis=0, tiled=True)
    down_part = lax.all_to_all(w_down, "g", split_axis=0, concat_axis=1, tiled=True)
    up_all = lax.all_gather(up_part, "z", axis=0, tiled=True)

    def turn(value, d):
        return lax.ppermute(value, "tp", [(i, (i + d) % tp) for i in range(tp)])

    w_out_parts = [w_out] + [turn(w_out, d) for d in range(1, tp)]
    segment = documents.astype(jnp.float32)
    decay_log = jax.nn.log_sigmoid(forget_gate)
    cumulative = jnp.cumsum(decay_log, axis=-1)
    key_heads = jnp.transpose(key_vectors.reshape(tok_rows, heads, head_dim), (1, 0, 2))
    value_heads = jnp.transpose(value_vectors.reshape(tok_rows, heads, head_dim), (1, 0, 2))
    query_heads = jnp.transpose(query_vectors.reshape(tok_rows, heads, head_dim), (1, 0, 2))
    query_heads = query_heads * jnp.asarray(head_dim ** (-0.5), query_heads.dtype)
    latest = segment == segment[-1]
    growth = jnp.where(latest[None, :], cumulative[:, -1:] - cumulative + in_gate, very_negative)
    top_log = jnp.max(growth, axis=-1)
    summary_weight = jnp.exp(growth - top_log[:, None])
    key_wide = key_heads.astype(jnp.float32)
    weighted = key_wide * summary_weight[:, :, None]
    memory = jnp.einsum(
        "hsv,hsk->hvk", value_heads.astype(jnp.float32), weighted, precision=lax.Precision.HIGHEST
    )
    normal = jnp.sum(weighted, axis=1)
    state = (
        jnp.concatenate([memory, normal[:, None, :]], axis=1),
        top_log,
        cumulative[:, -1],
        segment[0],
        segment[-1],
    )
    reach = min(length - 1, -(-(DOC_MOST - 1) // tok_rows))
    span = 1
    while span < reach:
        state = combine(shifted(state, span, length, here), state)
        span *= 2
    incoming = shifted(state, 1, length, here)
    memory_in, top_in, _, _, last_in = incoming
    row_ids = lax.broadcasted_iota(jnp.int32, (tok_rows, tok_rows), 0)
    col_ids = lax.broadcasted_iota(jnp.int32, (tok_rows, tok_rows), 1)
    allowed = (col_ids <= row_ids) & (segment[:, None] == segment[None, :])
    inside = jnp.where(
        allowed[None],
        cumulative[:, :, None] - cumulative[:, None, :] + in_gate[:, None, :],
        very_negative,
    )
    peak_inside = jnp.max(inside, axis=-1)
    scores = jnp.einsum("hld,hsd->hls", query_heads, key_heads, preferred_element_type=jnp.float32)
    weight_inside = jnp.exp(inside - peak_inside[:, :, None]) * scores
    from_block = jnp.einsum(
        "hls,hsv->hlv",
        weight_inside.astype(jnp.bfloat16),
        value_heads,
        preferred_element_type=jnp.float32,
    )
    sum_inside = jnp.sum(weight_inside, axis=-1)
    outside = jnp.where((segment == last_in)[None, :], cumulative + top_in[:, None], very_negative)
    peak_log = jnp.maximum(outside, peak_inside)
    carried = jnp.exp(outside - peak_log)
    local = jnp.exp(peak_inside - peak_log)
    readout = jnp.einsum(
        "hlk,hvk->hlv", query_heads.astype(jnp.float32), memory_in, precision=lax.Precision.HIGHEST
    )
    numer = carried[:, :, None] * readout[:, :, :head_dim] + local[:, :, None] * from_block
    denom = carried * readout[:, :, head_dim] + local * sum_inside
    mixed = numer / jnp.maximum(jnp.abs(denom), jnp.exp(-peak_log))[:, :, None]
    mixed = jnp.transpose(mixed, (1, 0, 2)).reshape(tok_rows, -1).astype(jnp.bfloat16)
    own_rows = tok_rows // tp
    mixed_rows = mixed.reshape(tp, own_rows, -1)
    projected = 0.0
    for d in range(tp):
        piece = lax.dynamic_index_in_dim(mixed_rows, (me + d) % tp, 0, keepdims=False)
        if d:
            piece = turn(piece, d)
        projected = projected + jnp.dot(piece, w_out_parts[d], preferred_element_type=jnp.float32)
    middle = (residual.astype(jnp.float32) + projected).astype(jnp.bfloat16)
    middle_wide = middle.astype(jnp.float32)
    factor = lax.rsqrt(jnp.mean(middle_wide * middle_wide, axis=-1, keepdims=True) + epsilon)
    normed = (middle_wide * factor * norm_gain.astype(jnp.float32)).astype(jnp.bfloat16)
    gathered = lax.all_gather(normed, ("g", "tp"), axis=0, tiled=True)
    down_all = lax.all_gather(down_part, "z", axis=1, tiled=True)
    lifted = jnp.dot(gathered, up_all, preferred_element_type=jnp.float32)
    hidden = jnp.square(jax.nn.relu(lifted)).astype(jnp.bfloat16)
    terms = jnp.dot(hidden, down_all, preferred_element_type=jnp.float32)
    summed = lax.psum_scatter(
        terms.astype(jnp.bfloat16), ("g", "tp"), scatter_dimension=0, tiled=True
    ).astype(jnp.float32)
    return (middle_wide + summed).astype(jnp.bfloat16)


def solution(mesh):
    sp, tp = (mesh.shape["sp"], mesh.shape["tp"])
    plane = min(sp, 2 * tp)
    if sp % plane:
        plane = 1
    split = Mesh(np.asarray(mesh.devices).reshape(sp // plane, plane, tp), ("z", "g", "tp"))
    placed = (
        P(("z", "g", "tp"), None),
        P(SP, "tp"),
        P(SP, "tp"),
        P(SP, "tp"),
        P("tp", SP),
        P("tp", SP),
        P(SP),
        P("tp", None),
        P(),
        P(SP, "tp"),
        P("tp", SP),
    )
    return jax.shard_map(
        on_device, mesh=split, in_specs=placed, out_specs=P(("z", "g", "tp"), None), check_vma=False
    )
```

profile of v0, /device:TPU:0, one launch (start us, length us, event | category | flops | bytes accessed | tf_op | source)
XLA Modules:
  0.0 308.7 jit_solution(7243872329865839913)
XLA Ops:
  6.6 18.8 %all_to_all.38 = bf16[4,1024,128]{2,1,0:T(8,128)(2,1)S(1)} all-to-all(bf16[4,1024,128]{2,1,0:T(8,128)(2,1)} %bitcast.89), channel_id=1, replica_groups=mesh['z'=4,'g'=4,'tp'=2] {'g'}, dimensions={0} | all-to-all | bytes 2097152 | tf_op jit(solution)/shard_map/all_to_all | solution.py:79
  25.4 1.4 copy.209
  27.5 0.6 pad.46.clone
  28.1 0.7 pad.47.clone
  28.9 1.2 reduce-window.6
  32.2 1.0 copy.193
  33.7 2.0 collective-permute-start
  35.7 1.3 copy.207
  37.0 4.7 %all-to-all-start = ((bf16[128,4,1024]{0,2,1:T(8,128)(2,1)}), bf16[128,4,1024]{0,2,1:T(8,128)(2,1)S(1)}, u32[]{:S(2)}, u32[]{:S(2)}) async-start(bf16[128,4,1024]{0,2,1:T(8,128)(2,1)} %bitcast.30), calls=%async_computation | async-start | bytes 2097152 | tf_op jit(solution)/shard_map/all_to_all | solution.py:78
  41.7 1.6 collective-permute-start.5
  45.3 1.1 slice_reduce_fusion.3
  46.3 0.7 fusion.46
  50.7 1.0 fusion.16
  51.8 3.9 %collective-permute-start.1 = (f32[4,72,64]{1,2,0:T(8,128)S(1)}, f32[4,72,64]{1,2,0:T(8,128)S(1)}, u32[]{:S(2)}, u32[]{:S(2)}) collective-permute-start(f32[4,72,64]{1,2,0:T(8,128)S(1)} %maximum_maximum_fusion.1), channel_id=1, source_target_pairs={{0,4},{2,6},{4,8},{6,10},{8,12},{10,14},{12,16},{14,18},{16,20},{1... | collective-permute-start | bytes 221192 | tf_op jit(solution)/shard_map/ppermute | solution.py:54
  56.1 3.0 collective-permute-done.1
  59.2 0.7 fusion.45
  60.5 1.3 copy.208
  63.3 8.0 %collective-permute-start.2 = (f32[4,72,64]{1,2,0:T(8,128)S(1)}, f32[4,72,64]{1,2,0:T(8,128)S(1)}, u32[]{:S(2)}, u32[]{:S(2)}) collective-permute-start(f32[4,72,64]{1,2,0:T(8,128)S(1)} %maximum_maximum_fusion.2), channel_id=1, source_target_pairs={{0,8},{2,10},{4,12},{6,14},{8,16},{10,18},{12,20},{14,22},{16,24},... | collective-permute-start | bytes 221192 | tf_op jit(solution)/shard_map/ppermute | solution.py:54
  71.9 5.7 %collective-permute-done.2 = f32[4,72,64]{1,2,0:T(8,128)S(1)} collective-permute-done((f32[4,72,64]{1,2,0:T(8,128)S(1)}, f32[4,72,64]{1,2,0:T(8,128)S(1)}, u32[]{:S(2)}, u32[]{:S(2)}) %collective-permute-start.2) | collective-permute-done | bytes 73760 | tf_op jit(solution)/shard_map/ppermute | solution.py:54
  77.7 0.7 fusion.44
  80.5 1.3 collective-permute-start.3
  81.9 0.9 collective-permute-done.3
  82.9 0.6 slice.113
  86.6 3.4 %collective-permute-done.4 = bf16[128,256]{1,0:T(8,128)(2,1)S(1)} collective-permute-done((bf16[128,256]{1,0:T(8,128)(2,1)S(1)}, bf16[128,256]{1,0:T(8,128)(2,1)S(1)}, u32[]{:S(2)}, u32[]{:S(2)}) %collective-permute-start.4) | collective-permute-done | bytes 65568 | tf_op jit(solution)/shard_map/ppermute | solution.py:83
  90.0 1.6 multiply_reduce_fusion
  91.6 1.0 multiply_convert_fusion.1
  92.7 16.1 %all-gather.8.cloned.1.call-done = bf16[1024,2048]{0,1:T(8,128)(2,1)} async-done(((bf16[1024,512]{0,1:T(8,128)(2,1)}), bf16[1024,2048]{0,1:T(8,128)(2,1)}) %all-gather.8.cloned.1.call-update) | async-done | bytes 4194320 | tf_op jit(solution)/shard_map/all_gather | solution.py:159
  108.7 88.8 %all-gather.6.cloned.1.call-done = bf16[2048,1024]{1,0:T(8,128)(2,1)} async-done(((bf16[512,1024]{1,0:T(8,128)(2,1)}), bf16[2048,1024]{1,0:T(8,128)(2,1)}) %all-gather.6.cloned.1.call-update) | async-done | bytes 4194320 | tf_op jit(solution)/shard_map/all_gather | solution.py:80
  197.6 37.0 %all-gather.4.cloned.1.call-done = bf16[1024,2048]{1,0:T(8,128)(2,1)} async-done(((bf16[128,2048]{1,0:T(8,128)(2,1)}), bf16[1024,2048]{1,0:T(8,128)(2,1)}) %all-gather.4.cloned.1.call-update) | async-done | bytes 4194320 | tf_op jit(solution)/shard_map/all_gather | solution.py:158
  234.6 14.4 %convolution_convert_fusion = bf16[1024,2048]{1,0:T(8,128)(2,1)} fusion(bf16[1024,2048]{0,1:T(8,128)(2,1)} %all-gather.8.cloned.1.call-done, bf16[1024,2048]{1,0:T(8,128)(2,1)} %all-gather.4.cloned.1.call-done, bf16[2048,1024]{1,0:T(8,128)(2,1)} %all-gather.6.cloned.1.call-done), kind=kOutput, calls=%fused_computation.1 | convolution fusion | flops 8595177472 | bytes 16777216 | tf_op jit(solution)/shard_map/dot_general | solution.py:162
  249.0 51.3 %reduce-scatter.2.cloned.1.call-done = bf16[128,2048]{1,0:T(8,128)(2,1)} async-done(((bf16[1024,2048]{1,0:T(8,128)(2,1)}), bf16[128,2048]{1,0:T(8,128)(2,1)}) %reduce-scatter.2.cloned.1.call-update) | async-done | bytes 524304 | tf_op jit(solution)/shard_map/reduce_scatter | solution.py:163
  300.3 1.9 add_convert_fusion
  (112 shorter events, 9.6 us)
Async XLA Ops:
  6.5 20.3 %copy-start.8 = (s32[256]{0:T(256)S(1)}, s32[256]{0:T(256)}, u32[]{:S(2)}) copy-start(s32[256]{0:T(256)} %param.17) | copy-start | bytes 3076
  6.5 22.3 %copy-start.10 = (f32[4,256]{1,0:T(4,128)S(1)}, f32[4,256]{1,0:T(4,128)}, u32[]{:S(2)}) copy-start(f32[4,256]{1,0:T(4,128)} %param.16) | copy-start | bytes 12292
  6.5 24.8 %copy-start.7 = (f32[4,256]{1,0:T(4,128)S(1)}, f32[4,256]{1,0:T(4,128)}, u32[]{:S(2)}) copy-start(f32[4,256]{1,0:T(4,128)} %param.15) | copy-start | bytes 12292
  6.5 25.2 %copy-start.5 = (bf16[256,256]{1,0:T(8,128)(2,1)S(1)}, bf16[256,256]{1,0:T(8,128)(2,1)}, u32[]{:S(2)}) copy-start(bf16[256,256]{1,0:T(8,128)(2,1)} %param.13) | copy-start | bytes 393220
  6.5 29.2 %copy-start = (bf16[128,4096]{1,0:T(8,128)(2,1)S(1)}, bf16[128,4096]{1,0:T(8,128)(2,1)}, u32[]{:S(2)}) copy-start(bf16[128,4096]{1,0:T(8,128)(2,1)} %param.20) | copy-start | bytes 3145732
  6.5 102.2 %all-gather.8.cloned.1.call-start = ((), (), s32[]{:S(2)}) async-start(), calls=%async_computation.5 | async-start | bytes 5242880 | tf_op jit(solution)/shard_map/all_gather | solution.py:159
  25.4 16.3 %copy-start.1 = (bf16[256,2048]{1,0:T(8,128)(2,1)S(1)}, bf16[256,2048]{1,0:T(8,128)(2,1)}, u32[]{:S(2)}) copy-start(bf16[256,2048]{1,0:T(8,128)(2,1)} %param.18) | copy-start | bytes 3145732
  26.8 16.5 %copy-start.6 = (bf16[256,256]{1,0:T(8,128)(2,1)S(1)}, bf16[256,256]{1,0:T(8,128)(2,1)}, u32[]{:S(2)}) copy-start(bf16[256,256]{1,0:T(8,128)(2,1)} %param.12) | copy-start | bytes 393220
  33.2 3.7 %copy-start.2 = (bf16[256,256]{0,1:T(8,128)(2,1)}, bf16[256,256]{0,1:T(8,128)(2,1)S(1)}, u32[]{:S(2)}) copy-start(bf16[256,256]{0,1:T(8,128)(2,1)S(1)} %copy.193) | copy-start | bytes 393220
  33.7 11.6 %collective-permute-start = (f32[4,72,64]{1,2,0:T(8,128)S(1)}, f32[4,72,64]{1,2,0:T(8,128)}, u32[]{:S(2)}, u32[]{:S(2)}) collective-permute-start(f32[4,72,64]{1,2,0:T(8,128)S(1)} %maximum_maximum_fusion), channel_id=1, source_target_pairs={{0,2},{2,4},{4,6},{6,8},{8,10},{10,12},{12,14},{14,16},{16,18},{18... | collective-permute-start | bytes 221192 | tf_op jit(solution)/shard_map/ppermute | solution.py:54
  37.0 23.5 %all-to-all-start = ((bf16[128,4,1024]{0,2,1:T(8,128)(2,1)}), bf16[128,4,1024]{0,2,1:T(8,128)(2,1)S(1)}, u32[]{:S(2)}, u32[]{:S(2)}) async-start(bf16[128,4,1024]{0,2,1:T(8,128)(2,1)} %bitcast.30), calls=%async_computation | async-start | bytes 2097152 | tf_op jit(solution)/shard_map/all_to_all | solution.py:78
  41.7 155.9 %all-gather.6.cloned.1.call-start = ((), (), s32[]{:S(2)}) async-start(), calls=%async_computation.4 | async-start | bytes 5242880 | tf_op jit(solution)/shard_map/all_gather | solution.py:80
  41.7 48.3 %collective-permute-start.5 = (bf16[256,2048]{1,0:T(8,128)(2,1)S(1)}, bf16[256,2048]{1,0:T(8,128)(2,1)}, u32[]{:S(2)}, u32[]{:S(2)}) collective-permute-start(bf16[256,2048]{1,0:T(8,128)(2,1)S(1)} %copy-done.1), channel_id=1, source_target_pairs={{0,1},{1,0},{2,3},{3,2},{4,5},{5,4},{6,7},{7,6},{8,9},{9,8},{10,11... | collective-permute-start | bytes 3145736 | tf_op jit(solution)/shard_map/ppermute | solution.py:83
  51.7 30.2 %copy-start.9 = (bf16[2048]{0:T(1024)(128)(2,1)S(1)}, bf16[2048]{0:T(1024)(128)(2,1)}, u32[]{:S(2)}) copy-start(bf16[2048]{0:T(1024)(128)(2,1)} %param.19) | copy-start | bytes 12292
  51.8 7.2 %collective-permute-start.1 = (f32[4,72,64]{1,2,0:T(8,128)S(1)}, f32[4,72,64]{1,2,0:T(8,128)S(1)}, u32[]{:S(2)}, u32[]{:S(2)}) collective-permute-start(f32[4,72,64]{1,2,0:T(8,128)S(1)} %maximum_maximum_fusion.1), channel_id=1, source_target_pairs={{0,4},{2,6},{4,8},{6,10},{8,12},{10,14},{12,16},{14,18},{16,20},{1... | collective-permute-start | bytes 221192 | tf_op jit(solution)/shard_map/ppermute | solution.py:54
  60.5 24.4 %copy-start.3 = (bf16[256,256]{0,1:T(8,128)(2,1)S(1)}, bf16[256,256]{0,1:T(8,128)(2,1)}, u32[]{:S(2)}) copy-start(bf16[256,256]{0,1:T(8,128)(2,1)} %copy-done.2) | copy-start | bytes 393220
  61.8 172.7 %all-gather.4.cloned.1.call-start = ((), (), s32[]{:S(2)}) async-start(), calls=%async_computation.3 | async-start | bytes 4718592 | tf_op jit(solution)/shard_map/all_gather | solution.py:158
  63.3 14.2 %collective-permute-start.2 = (f32[4,72,64]{1,2,0:T(8,128)S(1)}, f32[4,72,64]{1,2,0:T(8,128)S(1)}, u32[]{:S(2)}, u32[]{:S(2)}) collective-permute-start(f32[4,72,64]{1,2,0:T(8,128)S(1)} %maximum_maximum_fusion.2), channel_id=1, source_target_pairs={{0,8},{2,10},{4,12},{6,14},{8,16},{10,18},{12,20},{14,22},{16,24},... | collective-permute-start | bytes 221192 | tf_op jit(solution)/shard_map/ppermute | solution.py:54
  71.3 18.7 %copy-start.4 = (bf16[128,2048]{1,0:T(8,128)(2,1)S(1)}, bf16[128,2048]{1,0:T(8,128)(2,1)}, u32[]{:S(2)}) copy-start(bf16[128,2048]{1,0:T(8,128)(2,1)} %param.11) | copy-start | bytes 1572868
  80.5 2.3 collective-permute-start.3
  85.6 4.3 %collective-permute-start.4 = (bf16[128,256]{1,0:T(8,128)(2,1)S(1)}, bf16[128,256]{1,0:T(8,128)(2,1)S(1)}, u32[]{:S(2)}, u32[]{:S(2)}) collective-permute-start(bf16[128,256]{1,0:T(8,128)(2,1)S(1)} %bitcast.94), channel_id=1, source_target_pairs={{0,1},{1,0},{2,3},{3,2},{4,5},{5,4},{6,7},{7,6},{8,9},{9,8},{10,11... | collective-permute-start | bytes 196616 | tf_op jit(solution)/shard_map/ppermute | solution.py:83
  92.6 207.6 %reduce-scatter.2.cloned.1.call-start = ((), (), s32[]{:S(2)}) async-start(), calls=%async_computation.6 | async-start | bytes 4718592 | tf_op jit(solution)/shard_map/reduce_scatter | solution.py:163
Sparse Core Ops, SparseCore 0:
  26.9 81.7 all-gather.7
  110.3 87.2 all-gather.5
  199.5 35.0 all-gather.3
  249.1 51.1 reduce-scatter.1
where the time goes:
time: 309 us
  waiting for transfers between devices  206 us (67%)
  starting transfers between devices  22.2 us (7%)
  between operations  21.6 us (7%)
  blocking collectives  18.8 us (6%)
  matrix products  17.7 us (6%)
  local copies, waits for them, and re-layouts  13.7 us (4%)
  other arithmetic  8.61 us (3%)
    all_gather x1, waiting for transfers between devices, on_device(): up_all = lax.all_gather(up_part, 'z', axis=0, tiled=True)  88.8 us
    reduce_scatter x1, waiting for transfers between devices, on_device(): lax.psum_scatter(terms.astype(jnp.bfloat16), ('g', 'tp'), scatter_dimensi...  51.3 us
    all_gather x1, waiting for transfers between devices, on_device(): gathered = lax.all_gather(normed, ('g', 'tp'), axis=0, tiled=True)  37 us
    all_to_all x1, blocking collectives, on_device(): lax.all_to_all(w_down, 'g', split_axis=0, concat_axis=1, tiled=True)  18.8 us
    all_gather x1, waiting for transfers between devices, on_device(): down_all = lax.all_gather(down_part, 'z', axis=1, tiled=True)  16.1 us
    ppermute x4, starting transfers between devices, shifted(): lax.ppermute(pack(state), SP, [(i, i + distance) for i in range(length -...  15.2 us
    dot_general x1, matrix products, on_device(): terms = jnp.dot(hidden, down_all, preferred_element_type=jnp.float32)  14.4 us
    ppermute x4, waiting for transfers between devices, shifted(): lax.ppermute(pack(state), SP, [(i, i + distance) for i in range(length -...  9.54 us
  transfers between devices with their start and end apart: 11, of which 8 were waited for; matrix products, arithmetic and copies ran while one was open for 7% of the time, Pallas kernels for 0%

commit v1 on v0

--- a/solution.py
+++ b/solution.py
@@ -76,7 +76,10 @@
     tp = lax.axis_size("tp")
     me = lax.axis_index("tp")
     up_part = lax.all_to_all(w_up, "g", split_axis=1, concat_axis=0, tiled=True)
-    down_part = lax.all_to_all(w_down, "g", split_axis=0, concat_axis=1, tiled=True)
+    count = lax.axis_size("g")
+    blocks = jnp.stack(jnp.split(w_down, count, axis=0), axis=0)
+    blocks = lax.all_to_all(blocks, "g", split_axis=0, concat_axis=0)
+    down_part = jnp.concatenate(blocks, axis=1)
     up_all = lax.all_gather(up_part, "z", axis=0, tiled=True)
 
     def turn(value, d):

time: 309 us -> 310 us (level)
  waiting for transfers between devices: 206 us -> 199 us
  other arithmetic: 8.61 us -> 13.6 us
    all_gather x1, waiting for transfers between devices: 88.8 us -> 9.66 us  [on_device(): up_all = lax.all_gather(up_part, 'z', axis=0, tiled=True)]
    all_gather x1, waiting for transfers between devices: 16.1 us -> 88.8 us  [on_device(): down_all = lax.all_gather(down_part, 'z', axis=1, tiled=True)]
    unnamed x30 -> x56, local copies, waits for them, and re-layouts: 2.78 us -> 6.16 us
  transfers between devices with their start and end apart: 11 -> 11, of which waited for: 8 -> 8; matrix products, arithmetic and copies ran while one was open for 7% -> 9% of each run, Pallas kernels for 0% -> 0%
where the time goes in v1:
time: 310 us; the launch traced here: 309 us
  waiting for transfers between devices  199 us (64%)
  starting transfers between devices  21.6 us (7%)
  between operations  21.6 us (7%)
  matrix products  19.5 us (6%)
  blocking collectives  18.5 us (6%)
  local copies, waits for them, and re-layouts  15.6 us (5%)
  other arithmetic  13.6 us (4%)
    all_gather x1, waiting for transfers between devices, on_device(): down_all = lax.all_gather(down_part, 'z', axis=1, tiled=True)  88.8 us
    reduce_scatter x1, waiting for transfers between devices, on_device(): lax.psum_scatter(terms.astype(jnp.bfloat16), ('g', 'tp'), scatter_dimensi...  51.3 us
    all_gather x1, waiting for transfers between devices, on_device(): gathered = lax.all_gather(normed, ('g', 'tp'), axis=0, tiled=True)  37 us
    all_to_all x1, blocking collectives, on_device(): up_part = lax.all_to_all(w_up, 'g', split_axis=1, concat_axis=0, tiled=True)  18.5 us
    ppermute x4, starting transfers between devices, shifted(): lax.ppermute(pack(state), SP, [(i, i + distance) for i in range(length -...  15.4 us
    dot_general x1, matrix products, on_device(): terms = jnp.dot(hidden, down_all, preferred_element_type=jnp.float32)  14.4 us
    all_gather x1, waiting for transfers between devices, on_device(): up_all = lax.all_gather(up_part, 'z', axis=0, tiled=True)  9.66 us
    ppermute x4, waiting for transfers between devices, shifted(): lax.ppermute(pack(state), SP, [(i, i + distance) for i in range(length -...  8.69 us
  transfers between devices with their start and end apart: 11, of which 8 were waited for; matrix products, arithmetic and copies ran while one was open for 9% of the time, Pallas kernels for 0%

profile of v1, /device:TPU:0, one launch (start us, length us, event | category | flops | bytes accessed | tf_op | source)
XLA Modules:
  0.0 309.4 jit_solution(13836973348961497236)
XLA Ops:
  6.6 1.7 copy.229
  8.3 18.5 %all_to_all.24 = bf16[128,4,1024]{0,2,1:T(8,128)(2,1)S(1)} all-to-all(bf16[128,4,1024]{0,2,1:T(8,128)(2,1)S(1)} %bitcast.89), channel_id=1, replica_groups=mesh['z'=4,'g'=4,'tp'=2] {'g'}, dimensions={1} | all-to-all | bytes 2097152 | tf_op jit(solution)/shard_map/all_to_all | solution.py:78
  26.8 1.3 copy.230
  30.2 1.2 reduce-window.6
  35.4 0.8 maximum_maximum_fusion
  36.2 2.2 collective-permute-start
  39.0 1.1 pad_maximum_fusion
  40.1 3.9 %all-to-all-start.1 = ((bf16[4,1024,128]{1,2,0:T(8,128)(2,1)}), bf16[4,1024,128]{1,2,0:T(8,128)(2,1)S(1)}, u32[]{:S(2)}, u32[]{:S(2)}) async-start(bf16[4,1024,128]{1,2,0:T(8,128)(2,1)} %pad_maximum_fusion), calls=%async_computation.1 | async-start | bytes 2097152 | tf_op jit(solution)/shard_map/all_to_all | solution.py:81
  44.1 1.6 collective-permute-start.5
  45.7 1.0 copy.225
  46.7 0.8 fusion.9
  49.4 1.1 slice_reduce_fusion.3
  54.2 0.9 fusion.33
  56.6 1.0 fusion.16
  58.4 3.9 %collective-permute-start.1 = (f32[4,72,64]{1,2,0:T(8,128)S(1)}, f32[4,72,64]{1,2,0:T(8,128)S(1)}, u32[]{:S(2)}, u32[]{:S(2)}) collective-permute-start(f32[4,72,64]{1,2,0:T(8,128)S(1)} %maximum_maximum_fusion.1), channel_id=1, source_target_pairs={{0,4},{2,6},{4,8},{6,10},{8,12},{10,14},{12,16},{14,18},{16,20},{1... | collective-permute-start | bytes 221192 | tf_op jit(solution)/shard_map/ppermute | solution.py:54
  62.7 2.9 collective-permute-done.1
  67.0 1.0 copy-done
  69.5 8.1 %collective-permute-start.2 = (f32[4,72,64]{1,2,0:T(8,128)S(1)}, f32[4,72,64]{1,2,0:T(8,128)S(1)}, u32[]{:S(2)}, u32[]{:S(2)}) collective-permute-start(f32[4,72,64]{1,2,0:T(8,128)S(1)} %maximum_maximum_fusion.2), channel_id=1, source_target_pairs={{0,8},{2,10},{4,12},{6,14},{8,16},{10,18},{12,20},{14,22},{16,24},... | collective-permute-start | bytes 221192 | tf_op jit(solution)/shard_map/ppermute | solution.py:54
  77.5 1.3 fusion.49
  78.9 4.9 %collective-permute-done.2 = f32[4,72,64]{1,2,0:T(8,128)S(1)} collective-permute-done((f32[4,72,64]{1,2,0:T(8,128)S(1)}, f32[4,72,64]{1,2,0:T(8,128)S(1)}, u32[]{:S(2)}, u32[]{:S(2)}) %collective-permute-start.2) | collective-permute-done | bytes 73760 | tf_op jit(solution)/shard_map/ppermute | solution.py:54
  86.5 1.3 collective-permute-start.3
  87.9 0.9 collective-permute-done.3
  90.9 1.3 fusion.19
  93.6 3.5 %collective-permute-done.4 = bf16[128,256]{1,0:T(8,128)(2,1)S(1)} collective-permute-done((bf16[128,256]{1,0:T(8,128)(2,1)S(1)}, bf16[128,256]{1,0:T(8,128)(2,1)S(1)}, u32[]{:S(2)}, u32[]{:S(2)}) %collective-permute-start.4) | collective-permute-done | bytes 65568 | tf_op jit(solution)/shard_map/ppermute | solution.py:86
  97.1 1.6 multiply_reduce_fusion
  98.8 1.0 multiply_convert_fusion.1
  99.8 9.7 %all-gather.6.cloned.1.call-done = bf16[2048,1024]{1,0:T(8,128)(2,1)} async-done(((bf16[512,1024]{1,0:T(8,128)(2,1)}), bf16[2048,1024]{1,0:T(8,128)(2,1)}) %all-gather.6.cloned.1.call-update) | async-done | bytes 4194320 | tf_op jit(solution)/shard_map/all_gather | solution.py:83
  109.4 88.8 %all-gather.8.cloned.1.call-done = bf16[1024,2048]{0,1:T(8,128)(2,1)} async-done(((bf16[1024,512]{0,1:T(8,128)(2,1)}), bf16[1024,2048]{0,1:T(8,128)(2,1)}) %all-gather.8.cloned.1.call-update) | async-done | bytes 4194320 | tf_op jit(solution)/shard_map/all_gather | solution.py:162
  198.3 37.0 %all-gather.4.cloned.1.call-done = bf16[1024,2048]{1,0:T(8,128)(2,1)} async-done(((bf16[128,2048]{1,0:T(8,128)(2,1)}), bf16[1024,2048]{1,0:T(8,128)(2,1)}) %all-gather.4.cloned.1.call-update) | async-done | bytes 4194320 | tf_op jit(solution)/shard_map/all_gather | solution.py:161
  235.3 14.4 %convolution_convert_fusion = bf16[1024,2048]{1,0:T(8,128)(2,1)} fusion(bf16[1024,2048]{0,1:T(8,128)(2,1)} %all-gather.8.cloned.1.call-done, bf16[1024,2048]{1,0:T(8,128)(2,1)} %all-gather.4.cloned.1.call-done, bf16[2048,1024]{1,0:T(8,128)(2,1)} %all-gather.6.cloned.1.call-done), kind=kOutput, calls=%fused_computation.1 | convolution fusion | flops 8595177472 | bytes 16777216 | tf_op jit(solution)/shard_map/dot_general | solution.py:165
  249.7 51.3 %reduce-scatter.2.cloned.1.call-done = bf16[128,2048]{1,0:T(8,128)(2,1)} async-done(((bf16[1024,2048]{1,0:T(8,128)(2,1)}), bf16[128,2048]{1,0:T(8,128)(2,1)}) %reduce-scatter.2.cloned.1.call-update) | async-done | bytes 524304 | tf_op jit(solution)/shard_map/reduce_scatter | solution.py:166
  301.0 1.9 add_convert_fusion
  (139 shorter events, 16.1 us)
Async XLA Ops:
  6.5 21.7 %copy-start.15 = (s32[256]{0:T(256)S(1)}, s32[256]{0:T(256)}, u32[]{:S(2)}) copy-start(s32[256]{0:T(256)} %param.17) | copy-start | bytes 3076
  6.5 23.7 %copy-start.21 = (f32[4,256]{1,0:T(4,128)S(1)}, f32[4,256]{1,0:T(4,128)}, u32[]{:S(2)}) copy-start(f32[4,256]{1,0:T(4,128)} %param.16) | copy-start | bytes 12292
  6.5 26.6 %copy-start.8 = (f32[4,256]{1,0:T(4,128)S(1)}, f32[4,256]{1,0:T(4,128)}, u32[]{:S(2)}) copy-start(f32[4,256]{1,0:T(4,128)} %param.15) | copy-start | bytes 12292
  6.5 27.6 %copy-start.6 = (bf16[256,256]{1,0:T(8,128)(2,1)S(1)}, bf16[256,256]{1,0:T(8,128)(2,1)}, u32[]{:S(2)}) copy-start(bf16[256,256]{1,0:T(8,128)(2,1)} %param.13) | copy-start | bytes 393220
  6.5 28.0 %copy-start.7 = (bf16[256,256]{1,0:T(8,128)(2,1)S(1)}, bf16[256,256]{1,0:T(8,128)(2,1)}, u32[]{:S(2)}) copy-start(bf16[256,256]{1,0:T(8,128)(2,1)} %param.14) | copy-start | bytes 393220
  6.5 31.8 %copy-start.1 = (bf16[4096,128]{1,0:T(8,128)(2,1)S(1)}, bf16[4096,128]{1,0:T(8,128)(2,1)}, u32[]{:S(2)}) copy-start(bf16[4096,128]{1,0:T(8,128)(2,1)} %param.21) | copy-start | bytes 3145732
  6.6 102.9 %all-gather.6.cloned.1.call-start = ((), (), s32[]{:S(2)}) async-start(), calls=%async_computation.4 | async-start | bytes 5242880 | tf_op jit(solution)/shard_map/all_gather | solution.py:83
  28.2 3.5 %copy-start.12 = (f32[256]{0:T(256)}, f32[256]{0:T(256)S(1)}, u32[]{:S(2)}) copy-start(f32[256]{0:T(256)S(1)} %convert_element_type.54) | copy-start | bytes 3076
  28.3 6.7 %copy-start.17 = (f32[72]{0:T(128)}, f32[72]{0:T(128)S(1)}, u32[]{:S(2)}) copy-start(f32[72]{0:T(128)S(1)} %pad.47.clone) | copy-start | bytes 868
  33.2 1.3 copy-start.13
  33.4 1.0 copy-start.19
  33.5 0.6 copy-start.11
  34.7 0.7 copy-start.3
  36.2 7.9 %copy-start.2 = (bf16[256,2048]{1,0:T(8,128)(2,1)S(1)}, bf16[256,2048]{1,0:T(8,128)(2,1)}, u32[]{:S(2)}) copy-start(bf16[256,2048]{1,0:T(8,128)(2,1)} %param.18) | copy-start | bytes 3145732
  36.2 13.2 %collective-permute-start = (f32[4,72,64]{1,2,0:T(8,128)}, f32[4,72,64]{1,2,0:T(8,128)}, u32[]{:S(2)}, u32[]{:S(2)}) collective-permute-start(f32[4,72,64]{1,2,0:T(8,128)} %maximum_maximum_fusion), channel_id=1, source_target_pairs={{0,2},{2,4},{4,6},{6,8},{8,10},{10,12},{12,14},{14,16},{16,18},{18... | collective-permute-start | bytes 221192 | tf_op jit(solution)/shard_map/ppermute | solution.py:54
  38.7 30.5 %copy-start.14 = (f32[4]{0:T(128)S(1)}, f32[4]{0:T(128)}, u32[]{:S(2)}) copy-start(f32[4]{0:T(128)} %copy-done.13) | copy-start | bytes 52
  38.9 30.5 %copy-start.18 = (f32[72]{0:T(128)S(1)}, f32[72]{0:T(128)}, u32[]{:S(2)}) copy-start(f32[72]{0:T(128)} %copy-done.17) | copy-start | bytes 868
  40.1 26.9 %all-to-all-start.1 = ((bf16[4,1024,128]{1,2,0:T(8,128)(2,1)}), bf16[4,1024,128]{1,2,0:T(8,128)(2,1)S(1)}, u32[]{:S(2)}, u32[]{:S(2)}) async-start(bf16[4,1024,128]{1,2,0:T(8,128)(2,1)} %pad_maximum_fusion), calls=%async_computation.1 | async-start | bytes 2097152 | tf_op jit(solution)/shard_map/all_to_all | solution.py:81
  44.0 43.8 %copy-start.10 = (f32[4,2]{1,0:T(4,128)S(1)}, f32[4,2]{1,0:T(4,128)}, u32[]{:S(2)}) copy-start(f32[4,2]{1,0:T(4,128)} %copy-done.9) | copy-start | bytes 100
  44.0 43.9 %copy-start.20 = (bf16[2048]{0:T(1024)(128)(2,1)S(1)}, bf16[2048]{0:T(1024)(128)(2,1)}, u32[]{:S(2)}) copy-start(bf16[2048]{0:T(1024)(128)(2,1)} %param.19) | copy-start | bytes 12292
  44.0 46.3 %copy-start.16 = (s32[256]{0:T(256)S(1)}, s32[256]{0:T(256)}, u32[]{:S(2)}) copy-start(s32[256]{0:T(256)} %param.17) | copy-start | bytes 3076
  44.0 154.2 %all-gather.8.cloned.1.call-start = ((), (), s32[]{:S(2)}) async-start(), calls=%async_computation.5 | async-start | bytes 5242880 | tf_op jit(solution)/shard_map/all_gather | solution.py:162
  44.1 53.0 %collective-permute-start.5 = (bf16[256,2048]{1,0:T(8,128)(2,1)S(1)}, bf16[256,2048]{1,0:T(8,128)(2,1)}, u32[]{:S(2)}, u32[]{:S(2)}) collective-permute-start(bf16[256,2048]{1,0:T(8,128)(2,1)S(1)} %copy-done.2), channel_id=1, source_target_pairs={{0,1},{1,0},{2,3},{3,2},{4,5},{5,4},{6,7},{7,6},{8,9},{9,8},{10,11... | collective-permute-start | bytes 3145736 | tf_op jit(solution)/shard_map/ppermute | solution.py:86
  46.7 44.2 %copy-start.4 = (bf16[256,256]{0,1:T(8,128)(2,1)S(1)}, bf16[256,256]{0,1:T(8,128)(2,1)}, u32[]{:S(2)}) copy-start(bf16[256,256]{0,1:T(8,128)(2,1)} %copy-done.3) | copy-start | bytes 393220
  58.4 7.2 %collective-permute-start.1 = (f32[4,72,64]{1,2,0:T(8,128)S(1)}, f32[4,72,64]{1,2,0:T(8,128)S(1)}, u32[]{:S(2)}, u32[]{:S(2)}) collective-permute-start(f32[4,72,64]{1,2,0:T(8,128)S(1)} %maximum_maximum_fusion.1), channel_id=1, source_target_pairs={{0,4},{2,6},{4,8},{6,10},{8,12},{10,14},{12,16},{14,18},{16,20},{1... | collective-permute-start | bytes 221192 | tf_op jit(solution)/shard_map/ppermute | solution.py:54
  67.0 1.0 copy-start
  68.0 167.3 %all-gather.4.cloned.1.call-start = ((), (), s32[]{:S(2)}) async-start(), calls=%async_computation.3 | async-start | bytes 4718592 | tf_op jit(solution)/shard_map/all_gather | solution.py:161
  69.5 14.3 %collective-permute-start.2 = (f32[4,72,64]{1,2,0:T(8,128)S(1)}, f32[4,72,64]{1,2,0:T(8,128)S(1)}, u32[]{:S(2)}, u32[]{:S(2)}) collective-permute-start(f32[4,72,64]{1,2,0:T(8,128)S(1)} %maximum_maximum_fusion.2), channel_id=1, source_target_pairs={{0,8},{2,10},{4,12},{6,14},{8,16},{10,18},{12,20},{14,22},{16,24},... | collective-permute-start | bytes 221192 | tf_op jit(solution)/shard_map/ppermute | solution.py:54
  77.5 19.6 %copy-start.5 = (bf16[128,2048]{1,0:T(8,128)(2,1)S(1)}, bf16[128,2048]{1,0:T(8,128)(2,1)}, u32[]{:S(2)}) copy-start(bf16[128,2048]{1,0:T(8,128)(2,1)} %param.11) | copy-start | bytes 1572868
  86.5 2.3 collective-permute-start.3
  92.8 4.3 %collective-permute-start.4 = (bf16[128,256]{1,0:T(8,128)(2,1)S(1)}, bf16[128,256]{1,0:T(8,128)(2,1)S(1)}, u32[]{:S(2)}, u32[]{:S(2)}) collective-permute-start(bf16[128,256]{1,0:T(8,128)(2,1)S(1)} %bitcast.101), channel_id=1, source_target_pairs={{0,1},{1,0},{2,3},{3,2},{4,5},{5,4},{6,7},{7,6},{8,9},{9,8},{10,11... | collective-permute-start | bytes 196616 | tf_op jit(solution)/shard_map/ppermute | solution.py:86
  99.7 201.2 %reduce-scatter.2.cloned.1.call-start = ((), (), s32[]{:S(2)}) async-start(), calls=%async_computation.6 | async-start | bytes 4718592 | tf_op jit(solution)/shard_map/reduce_scatter | solution.py:166
  (1 other events, 0.5 us)
Sparse Core Ops, SparseCore 0:
  28.3 81.0 all-gather.5
  111.0 87.2 all-gather.7
  200.2 35.0 all-gather.3
  249.8 51.1 reduce-scatter.1
